TPU v7x, 128 devices: a whole 4x4x4 slice. The times are simulated.
128 devices in a mesh: sp: 16 (over z, y), fs: 4 (over x), tp: 2 (over core).
Axes of the slice: x: 4, y: 4, z: 4, core: 2. Of those that a mesh axis runs over, the one named last changes fastest.
Arguments:
- hidden_in: bfloat16 [32768, 2048], P(('fs', 'sp'), 'tp'), parts along dimension 0, may hold values from -6 to 48
- in_gain: float32 [2048], replicated, may hold values from 0.1 to 1.9
- w_query: bfloat16 [2048, 1024], P(None, 'tp'), may hold values from -0.29972302 to 0.29972302
- w_key: bfloat16 [2048, 1024], P(None, 'tp'), may hold values from -0.29972302 to 0.29972302
- w_value: bfloat16 [2048, 1024], P(None, 'tp'), may hold values from -0.125 to 0.125
- w_gate: bfloat16 [2048, 1024], P(None, 'tp'), may hold values from -0.125 to 0.125
- w_inner: bfloat16 [2048, 1024], P(None, 'tp'), may hold values from -0.125 to 0.125
- w_bvec: bfloat16 [2048, 512], P(None, 'tp'), may hold values from -0.125 to 0.125
- w_cvec: bfloat16 [2048, 512], P(None, 'tp'), may hold values from -0.125 to 0.125
- w_step: bfloat16 [2048, 16], P(None, 'tp'), may hold values from -0.125 to 0.125
- conv_inner: bfloat16 [4, 1024], P(None, 'tp'), may hold values from -3 to 3
- conv_bvec: bfloat16 [4, 512], P(None, 'tp'), may hold values from -3 to 3
- conv_cvec: bfloat16 [4, 512], P(None, 'tp'), may hold values from -3 to 3
- a_log: float32 [16], P('tp'), may hold values from -16 to 0
- decay_add: float32 [32768, 16], P(('fs', 'sp'), 'tp'), parts along dimension 0, may hold values from -1 to 0
- lambdas: float32 [4], P('tp'), may hold values from 0.3 to 0.8
- head_gain: float32 [256], replicated, may hold values from 0.1 to 1.9
- ssm_gain: float32 [1024], P('tp'), may hold values from 0.1 to 1.9
- out_attn: bfloat16 [1024, 2048], P('tp'), may hold values from -0.125 to 0.125
- out_ssm: bfloat16 [1024, 2048], P('tp'), may hold values from -0.125 to 0.125
Outputs:
- layer_out: bfloat16 [32768, 2048], P(('fs', 'sp', 'tp')), parts along dimension 0
There are 4 independent parts, one for each index of `fs`. A program takes and returns all parts, laid end to end along the dimension named above; an argument that names none is the same for every part. Nothing has to cross between parts.
All inputs are finite; a program needn't handle non-finite values.
Results may differ from a plain program's by a relative error of at most 0.012.
The roundings to bfloat16 on the way count: a program that leaves them out, or rounds other values in their place, can miss the bound.
Values may be sent and summed in bfloat16 or wider, within the bound.
A program may use at most 128 MiB of HBM per device.

v0:
```python
import jax
import jax.numpy as jnp
from jax import lax
from jax.sharding import Mesh
from jax.sharding import PartitionSpec as P

D = 2048
QK_DIM = 128
SSM_P = 64
STATE = 128
BLOCK = 128
KEY_BLOCK = 128
SP = ("sp_0", "sp_1")
FS_SP = ("fs", "sp_0", "sp_1")
FS_SP_TP = ("fs", "sp_0", "sp_1", "tp")
EPS = 1e-06
NEG = -1e30


def gathered_total(x, axis):
    return lax.all_gather(x, axis).sum(0)


def laid_out(parts, dim):
    lengths = list(parts.shape[1:])
    lengths[dim] *= parts.shape[0]
    return jnp.moveaxis(parts, 0, dim).reshape(lengths)


def copy_for_each(x, axis):
    length = lax.axis_size(axis)
    return lax.all_to_all(jnp.broadcast_to(x[None], (length, *x.shape)), axis, 0, 0, tiled=True)


def collect(x, axis, dim):
    return laid_out(copy_for_each(x, axis), dim)


def from_behind(x, axis, by):
    length = lax.axis_size(axis)
    pairs = [(i, i + by) for i in range(length) if 0 <= i + by < length]
    return lax.ppermute(x, axis, pairs)


def nothing_yet(x, identity):
    return jax.tree.map(
        lambda a, e: jnp.broadcast_to(jnp.asarray(e, a.dtype), a.shape), x, identity
    )


def prefix_by_axis(x, axes, combine, identity):
    before = start = nothing_yet(x, identity)
    running = x
    for axis in reversed(axes):
        length, index = (lax.axis_size(axis), lax.axis_index(axis))
        pieces = jax.tree.map(
            lambda part, kind: lax.all_gather(part.astype(kind), axis),
            running,
            (jnp.bfloat16, jnp.bfloat16),
        )
        inside, running = (start, start)
        for k in range(length):
            passed = k < index
            running = combine(
                running, jax.tree.map(lambda part, own: part[k].astype(own.dtype), pieces, x)
            )
            inside = jax.tree.map(lambda new, old: jnp.where(passed, new, old), running, inside)
        before = combine(inside, before)
    return before


def side_by_side(arrays, axis, dim, along):
    both = jnp.concatenate(arrays, axis=along)
    filled, at, gathered = (lax.all_gather(both, axis, axis=dim, tiled=True), 0, [])
    for a in arrays:
        gathered.append(lax.slice_in_dim(filled, at, at + a.shape[along], axis=along))
        at += a.shape[along]
    return tuple(gathered)


def per_device(
    hidden_in,
    in_gain,
    w_query,
    w_key,
    w_value,
    w_gate,
    w_inner,
    w_bvec,
    w_cvec,
    w_step,
    conv_inner,
    conv_bvec,
    conv_cvec,
    a_log,
    decay_add,
    lambdas,
    head_gain,
    ssm_gain,
    out_attn,
    out_ssm,
):
    rows_dev, half_width = hidden_in.shape
    in_float = hidden_in.astype(jnp.float32)
    squares = gathered_total(jnp.sum(in_float * in_float, axis=1), "tp")
    gain_half = lax.dynamic_slice_in_dim(in_gain, lax.axis_index("tp") * half_width, half_width, 0)
    normed = (in_float * lax.rsqrt(squares[:, None] / D + EPS) * gain_half[None, :]).astype(
        jnp.bfloat16
    )
    whole = collect(normed, "tp", 1)
    weight_list = (w_query, w_key, w_value, w_gate, w_inner, w_bvec, w_cvec, w_step)
    query, keys, values, gate_z, inner, b_pre, c_pre, step_pre = [
        jnp.dot(whole, weight, preferred_element_type=jnp.float32).astype(jnp.bfloat16)
        for weight in weight_list
    ]
    heads_att = lambdas.shape[0]
    first_row = lax.axis_index(SP) * rows_dev
    own_pos = first_row + jnp.arange(rows_dev, dtype=jnp.int32)
    scale = QK_DIM ** (-0.5)

    def head_major(rows_mat):
        return rows_mat.reshape(rows_mat.shape[0], heads_att * 2, QK_DIM).transpose(1, 0, 2)

    keys_major = head_major(keys)
    values_major = values.reshape(rows_dev, heads_att, 2 * QK_DIM).transpose(1, 0, 2)
    groups = [(head_major(query), own_pos)]
    start_states = tuple(
        (
            (
                jnp.full((heads_att, 2, group_pos.shape[0]), NEG, jnp.float32),
                jnp.zeros((heads_att, 2, group_pos.shape[0]), jnp.float32),
                jnp.zeros((heads_att, 2, group_pos.shape[0], 2 * QK_DIM), jnp.float32),
            )
            for group_query, group_pos in groups
        )
    )
    key_piece = lax.all_gather(keys_major, SP, axis=1, tiled=True)
    value_piece = lax.all_gather(values_major, SP, axis=1, tiled=True)

    def one_block(block_index, states):
        key_start = block_index * KEY_BLOCK
        key_rows = lax.dynamic_slice_in_dim(key_piece, block_index * KEY_BLOCK, KEY_BLOCK, 1)
        value_rows = lax.dynamic_slice_in_dim(value_piece, block_index * KEY_BLOCK, KEY_BLOCK, 1)
        key_pos = key_start + jnp.arange(KEY_BLOCK, dtype=jnp.int32)
        results = []
        for (group_query, group_pos), state in zip(groups, states):
            query_count = group_pos.shape[0]

            def update(current):
                peak, totals, accum = current
                scores = (
                    jnp.einsum(
                        "mqd,mkd->mqk", group_query, key_rows, preferred_element_type=jnp.float32
                    ).reshape(heads_att, 2, query_count, KEY_BLOCK)
                    * scale
                )
                visible = (key_pos[None, :] <= group_pos[:, None])[None, None]
                new_peak = jnp.maximum(peak, jnp.max(jnp.where(visible, scores, NEG), axis=-1))
                weights = jnp.where(visible, jnp.exp(scores - new_peak[..., None]), 0.0)
                shrink = jnp.exp(peak - new_peak)
                totals = totals * shrink + jnp.sum(weights, axis=-1)
                accum = accum * shrink[..., None] + jnp.einsum(
                    "hmqk,hke->hmqe",
                    weights.astype(jnp.bfloat16),
                    value_rows,
                    preferred_element_type=jnp.float32,
                )
                return (new_peak, totals, accum)

            results.append(
                lax.cond(key_start <= group_pos[-1], update, lambda unchanged: unchanged, state)
            )
        return tuple(results)

    finals = lax.fori_loop(0, key_piece.shape[1] // KEY_BLOCK, one_block, start_states)
    outputs = []
    for peak, totals, accum in finals:
        first_map = accum[:, 0] / totals[:, 0, :, None]
        second_map = accum[:, 1] / totals[:, 1, :, None]
        differ = first_map - lambdas[:, None, None] * second_map
        head_norm = (
            differ * lax.rsqrt(jnp.mean(differ * differ, axis=-1, keepdims=True) + EPS) * head_gain
        )
        outputs.append(
            head_norm.astype(jnp.bfloat16)
            .transpose(1, 0, 2)
            .reshape(accum.shape[2], heads_att * 2 * QK_DIM)
        )
    attn_out = outputs[0]
    heads_ssm = a_log.shape[0]
    groups_local = b_pre.shape[1] // STATE
    per_group = heads_ssm // groups_local
    stacked = jnp.concatenate([inner, b_pre, c_pre], axis=1)
    taps = conv_inner.shape[0]
    earlier = from_behind(stacked[rows_dev - (taps - 1) :], SP, 1)
    padded = jnp.concatenate([earlier, stacked], axis=0).astype(jnp.float32)
    conv_weight = jnp.concatenate([conv_inner, conv_bvec, conv_cvec], axis=1).astype(jnp.float32)
    summed = padded[0:rows_dev] * conv_weight[0]
    for offset in range(1, taps):
        summed = summed + padded[offset : offset + rows_dev] * conv_weight[offset]
    activated = jax.nn.silu(summed).astype(jnp.bfloat16)
    width_inner = inner.shape[1]
    width_vec = b_pre.shape[1]
    block_count = rows_dev // BLOCK
    inputs_x = activated[:, :width_inner].reshape(block_count, BLOCK, heads_ssm, SSM_P)
    inputs_b = activated[:, width_inner : width_inner + width_vec].reshape(
        block_count, BLOCK, groups_local, STATE
    )
    inputs_c = activated[:, width_inner + width_vec :].reshape(
        block_count, BLOCK, groups_local, STATE
    )
    step_size = jax.nn.softplus(step_pre.astype(jnp.float32))
    log_decay = -jnp.exp(a_log)[None, :] * step_size + decay_add
    size_major = step_size.reshape(block_count, BLOCK, heads_ssm).transpose(0, 2, 1)
    running = jnp.cumsum(
        log_decay.reshape(block_count, BLOCK, heads_ssm).transpose(0, 2, 1), axis=2
    )
    causal = jnp.tril(jnp.ones((BLOCK, BLOCK), dtype=bool))
    decay = jnp.exp(
        jnp.where(causal[None, None], running[:, :, :, None] - running[:, :, None, :], NEG)
    )
    intersection = jnp.einsum(
        "ntgk,nsgk->ngts", inputs_c, inputs_b, preferred_element_type=jnp.float32
    )
    matrix = (
        jnp.repeat(intersection, per_group, axis=1) * decay * size_major[:, :, None, :]
    ).astype(jnp.bfloat16)
    inside = jnp.einsum("nhts,nshp->nthp", matrix, inputs_x, preferred_element_type=jnp.float32)
    to_end = (jnp.exp(running[:, :, -1:] - running) * size_major).transpose(0, 2, 1)
    weighted = (inputs_x.astype(jnp.float32) * to_end[..., None]).astype(jnp.bfloat16)
    heads_b = jnp.repeat(inputs_b, per_group, axis=2)
    fresh = jnp.einsum("nshp,nshk->nhpk", weighted, heads_b, preferred_element_type=jnp.float32)
    block_totals = running[:, :, -1]

    def chain(state, items):
        fresh_block, total_block = items
        return (state * jnp.exp(total_block)[:, None, None] + fresh_block, state)

    local_end, local_enter = lax.scan(
        chain, jnp.zeros((heads_ssm, SSM_P, STATE), jnp.float32), (fresh, block_totals)
    )
    device_total = jnp.sum(block_totals, axis=0)

    def link(before, after):
        return (before[0] * jnp.exp(after[1])[:, None, None] + after[0], before[1] + after[1])

    incoming, skipped = prefix_by_axis(
        (local_end, device_total),
        SP,
        link,
        (jnp.zeros_like(local_end), jnp.zeros_like(device_total)),
    )
    preceding = jnp.concatenate(
        [jnp.zeros((1, heads_ssm), jnp.float32), jnp.cumsum(block_totals, axis=0)[:-1]], axis=0
    )
    entering = local_enter + incoming[None] * jnp.exp(preceding)[:, :, None, None]
    heads_c = jnp.repeat(inputs_c, per_group, axis=2).astype(jnp.float32)
    carried = (
        jnp.einsum("nthk,nhpk->nthp", heads_c, entering, precision=lax.Precision.HIGHEST)
        * jnp.exp(running).transpose(0, 2, 1)[..., None]
    )
    ssm_y = (inside + carried).reshape(rows_dev, heads_ssm * SSM_P)
    gated = (ssm_y * jax.nn.silu(gate_z.astype(jnp.float32))).reshape(rows_dev, groups_local, -1)
    grouped = gated * lax.rsqrt(jnp.mean(gated * gated, axis=-1, keepdims=True) + EPS)
    ssm_out = (grouped.reshape(rows_dev, heads_ssm * SSM_P) * ssm_gain).astype(jnp.bfloat16)
    attn_rows, ssm_rows = (
        lax.all_to_all(attn_out, "tp", split_axis=0, concat_axis=1, tiled=True),
        lax.all_to_all(ssm_out, "tp", split_axis=0, concat_axis=1, tiled=True),
    )
    full_attn, full_ssm = side_by_side((out_attn, out_ssm), "tp", 0, 1)
    joined = jnp.dot(attn_rows, full_attn, preferred_element_type=jnp.float32) + jnp.dot(
        ssm_rows, full_ssm, preferred_element_type=jnp.float32
    )
    return joined.astype(jnp.bfloat16)


def solution(mesh):
    split = Mesh(
        mesh.devices.reshape(4, 4, mesh.shape["fs"], mesh.shape["tp"]), ("sp_0", "sp_1", "fs", "tp")
    )
    in_specs = (
        P(FS_SP, "tp"),
        P(),
        P(None, "tp"),
        P(None, "tp"),
        P(None, "tp"),
        P(None, "tp"),
        P(None, "tp"),
        P(None, "tp"),
        P(None, "tp"),
        P(None, "tp"),
        P(None, "tp"),
        P(None, "tp"),
        P(None, "tp"),
        P("tp"),
        P(FS_SP, "tp"),
        P("tp"),
        P(),
        P("tp"),
        P("tp", None),
        P("tp", None),
    )
    out_specs = P(FS_SP_TP, None)
    return jax.shard_map(
        per_device, mesh=split, in_specs=in_specs, out_specs=out_specs, check_vma=False
    )
```

profile of v0, /device:TPU:127, one launch (start us, length us, event | category | flops | bytes accessed | tf_op | source)
XLA Modules:
  0.0 632.4 jit_solution(1211561122861284005)
XLA Ops:
  18.1 5.5 all_to_all.43
  43.7 7.7 %all-reduce.1 = bf16[32]{0:T(256)(128)(2,1)S(1)} all-reduce(bf16[32]{0:T(256)(128)(2,1)S(1)} %dynamic-update-slice), channel_id=3, replica_groups=mesh['sp_0'=4,'sp_1'=4,'fs'=4,'tp'=2] {'sp_1'}, use_global_device_ids=true, to_apply=%add.1 | all-reduce | flops 32 | bytes 128
  77.0 7.2 %while.31 = (s32[]{:T(128)}, f32[8,64,128]{2,1,0:T(8,128)S(1)}, f32[4,8,64,128]{3,2,1,0:T(8,128)}, f32[4,8]{1,0:T(4,128)S(1)}, f32[4,8,64,128]{3,2,1,0:T(8,128)}, /*index=5*/s32[]{:T(128)}, s32[]{:T(128)}) while((s32[]{:T(128)}, f32[8,64,128]{2,1,0:T(8,128)S(1)}, f32[4,8,64,128]{3,2,1,0:T(8,128)}, f32[4,8]{1,0:T(4,128)S(1)}, ...), condition=%wide.region_11.12_spmd.clone, body=%wide.region_10.11_spmd.clone.sunk | while | flops 262147 | bytes 1311424 | solution.py:239
  85.5 14.2 %all-gather.2 = bf16[32,64,128]{2,1,0:T(8,128)(2,1)S(1)} all-gather(bf16[8,64,128]{2,1,0:T(8,128)(2,1)S(1)} %convert_element_type.242), channel_id=4, replica_groups=mesh['sp_0'=4,'sp_1'=4,'fs'=4,'tp'=2] {'sp_1'}, dimensions={0}, use_global_device_ids=true | all-gather | bytes 655360 | tf_op jit(solution)/shard_map/all_gather | solution.py:57
  100.6 12.0 %all_gather.42 = bf16[4,8,64,128]{3,2,1,0:T(8,128)(2,1)S(1)} all-gather(bf16[1,8,64,128]{3,2,1,0:T(8,128)(2,1)S(1)} %fusion.62), channel_id=1, replica_groups=mesh['sp_0'=4,'sp_1'=4,'fs'=4,'tp'=2] {'sp_0'}, dimensions={0}, use_global_device_ids=true | all-gather | bytes 655360 | tf_op jit(solution)/shard_map/all_gather | solution.py:57
  134.0 10.5 %all_to_all.44 = bf16[2,256,512]{1,2,0:T(8,128)(2,1)S(1)} all-to-all(bf16[2,256,512]{1,2,0:T(8,128)(2,1)S(1)} %copy.107), channel_id=1, replica_groups=mesh['sp_0'=4,'sp_1'=4,'fs'=4,'tp'=2] {'tp'}, dimensions={0} | all-to-all | bytes 1048576 | tf_op jit(solution)/shard_map/all_to_all | solution.py:268
  149.3 34.8 %all-gather.9.cloned.1.call-done = bf16[4,8192,128]{2,1,0:T(8,128)(2,1)} async-done(((bf16[4,512,128]{2,1,0:T(8,128)(2,1)}), bf16[4,8192,128]{2,1,0:T(8,128)(2,1)}) %all-gather.9.cloned.1.call-update) | async-done | bytes 8388624 | tf_op jit(solution)/shard_map/all_gather | solution.py:137
  185.7 426.3 %while.30 = (s32[]{:T(128)}, f32[2,2,512]{2,1,0:T(2,128)S(1)}, f32[2,2,512]{2,1,0:T(2,128)S(1)}, f32[2,2,512,256]{3,2,1,0:T(8,128)}, s32[512]{0:T(512)S(1)}, /*i...) while((s32[]{:T(128)}, f32[2,2,512]{2,1,0:T(2,128)S(1)}, ...), condition=%wide.region_7.8_spmd, body=%wide.region_2.7_spmd.sunk | while | flops 204804224 | bytes 10801461 | solution.py:175
  213.8 5.3 conditional.2
  233.7 5.3 conditional.2
  253.7 5.3 conditional.2
  267.0 5.3 conditional.2
  287.0 5.3 conditional.2
  307.0 5.3 conditional.2
  340.3 5.3 conditional.2
  360.3 5.3 conditional.2
  380.3 5.3 conditional.2
  393.6 5.3 conditional.2
  413.6 5.3 conditional.2
  433.6 5.3 conditional.2
  466.9 5.3 conditional.2
  486.9 5.3 conditional.2
  506.8 5.3 conditional.2
  520.2 5.3 conditional.2
  (1174 shorter events, 738.2 us)
Async XLA Ops:
  6.5 118.4 %copy-start = (bf16[2048,512]{1,0:T(8,128)(2,1)S(1)}, bf16[2048,512]{1,0:T(8,128)(2,1)}, u32[]{:S(2)}) copy-start(bf16[2048,512]{1,0:T(8,128)(2,1)} %param.31) | copy-start | bytes 6291460
  6.5 138.0 %all-gather.13.cloned.1.call-start = ((), (), s32[]{:S(2)}) async-start(), calls=%async_computation.5 | async-start | bytes 12582912 | tf_op jit(solution)/shard_map/all_gather | solution.py:74
  11.4 137.9 %all-gather.11.cloned.1.call-start = ((), (), s32[]{:S(2)}) async-start(), calls=%async_computation.4 | async-start | bytes 8912896 | tf_op jit(solution)/shard_map/all_gather | solution.py:138
  18.0 6.9 %copy-start.25 = (bf16[2048,512]{1,0:T(8,128)(2,1)S(1)}, bf16[2048,512]{1,0:T(8,128)(2,1)}, u32[]{:S(2)}) copy-start(bf16[2048,512]{1,0:T(8,128)(2,1)} %param.30) | copy-start | bytes 6291460
  23.6 1.3 copy-start.2
  27.3 156.8 %all-gather.9.cloned.1.call-start = ((), (), s32[]{:S(2)}) async-start(), calls=%async_computation.3 | async-start | bytes 8912896 | tf_op jit(solution)/shard_map/all_gather | solution.py:137
  32.3 2.8 copy-start.3
  32.4 2.8 copy-start.27
  35.2 3.0 copy-start.8
  35.2 1.7 copy-start.26
  36.9 1.3 copy-start.9
  36.9 3.5 copy-start.28
  36.9 3.5 copy-start.14
  38.2 2.6 copy-start.15
  38.2 3.8 copy-start.29
  38.2 19.7 %copy-start.18 = (bf16[4,512]{1,0:T(4,128)(2,1)S(1)}, bf16[4,512]{1,0:T(4,128)(2,1)}, u32[]{:S(2)}) copy-start(bf16[4,512]{1,0:T(4,128)(2,1)} %param.36) | copy-start | bytes 12292
  38.2 19.7 %copy-start.19 = (bf16[4,256]{1,0:T(4,128)(2,1)S(1)}, bf16[4,256]{1,0:T(4,128)(2,1)}, u32[]{:S(2)}) copy-start(bf16[4,256]{1,0:T(4,128)(2,1)} %param.38) | copy-start | bytes 6148
  38.2 19.7 %copy-start.20 = (bf16[4,256]{1,0:T(4,128)(2,1)S(1)}, bf16[4,256]{1,0:T(4,128)(2,1)}, u32[]{:S(2)}) copy-start(bf16[4,256]{1,0:T(4,128)(2,1)} %param.37) | copy-start | bytes 6148
  39.1 27.0 %collective-permute-start = (bf16[3,1024]{0,1:T(8,128)(2,1)}, bf16[3,1024]{0,1:T(8,128)(2,1)}, u32[]{:S(2)}, u32[]{:S(2)}) collective-permute-start(bf16[3,1024]{0,1:T(8,128)(2,1)} %pad_maximum_fusion.1), channel_id=1, source_target_pairs={{0,8},{8,16},{16,24},{24,32},{32,40},{40,48},{48,56},{56,64},{64,7... | collective-permute-start | bytes 18440 | tf_op jit(solution)/shard_map/ppermute | solution.py:42
  40.8 23.4 %copy-start.10 = (f32[512,8]{0,1:T(8,128)}, f32[512,8]{0,1:T(8,128)S(1)}, u32[]{:S(2)}) copy-start(f32[512,8]{0,1:T(8,128)S(1)} %compare_select_fusion) | copy-start | bytes 49156
  149.3 36.4 %copy-start.12 = (s32[512]{0:T(512)S(1)}, s32[512]{0:T(512)}, u32[]{:S(2)}) copy-start(s32[512]{0:T(512)} %iota_add_fusion) | copy-start | bytes 6148
  185.7 426.4 %copy-start.24 = (f32[2]{0:T(128)S(1)}, f32[2]{0:T(128)}, u32[]{:S(2)}) copy-start(f32[2]{0:T(128)} %param.41) | copy-start | bytes 28
  612.1 2.1 copy-start.23
  620.6 5.3 copy-start.1
  (10 other events, 11.2 us)
Sparse Core Ops, SparseCore 0:
  11.5 24.0 all-gather.12
  37.8 73.6 all-gather.10
  113.6 70.4 all-gather.8
where the time goes:
time: 637 us; the launch traced here: 632 us
  matrix products  313 us (49%)
  local copies, waits for them, and re-layouts  106 us (17%)
  blocking collectives  62.5 us (10%)
  other arithmetic  50.5 us (8%)
  loops' own time  49.6 us (8%)
  waiting for transfers between devices  34.9 us (5%)
  between operations  14.3 us (2%)
    dot_general x64, matrix products, update(): jnp.einsum('hmqk,hke->hmqe', weights.astype(jnp.bfloat16), value_rows, pr...  196 us
    dot_general x64, matrix products, update(): jnp.einsum('mqd,mkd->mqk', group_query, key_rows, preferred_element_type=...  80.3 us
    another operation x1, loops' own time, per_device(): lax.fori_loop(0, key_piece.shape[1] // KEY_BLOCK, one_block, start_states)  44.8 us
    slice x64, local copies, waits for them, and re-layouts, one_block(): group_pos[-1]  42.2 us
    all_gather x1, waiting for transfers between devices, per_device(): key_piece = lax.all_gather(keys_major, SP, axis=1, tiled=True)  34.8 us
    all_gather x3, blocking collectives, prefix_by_axis(): lax.all_gather(part.astype(kind), axis)  31.5 us
    mul x64, local copies, waits for them, and re-layouts, update(): jnp.einsum('mqd,mkd->mqk', group_query, key_rows, preferred_element_type=...  20.7 us
    dot_general x8, matrix products, per_device(): jnp.dot(whole, weight, preferred_element_type=jnp.float32)  19.7 us
  transfers between devices with their start and end apart: 4, of which 1 were waited for; matrix products, arithmetic and copies ran while one was open for 12% of the time, Pallas kernels for 0%

commit v1 on v0

--- a/solution.py
+++ b/solution.py
@@ -134,7 +134,9 @@
             for group_query, group_pos in groups
         )
     )
-    key_piece = lax.all_gather(keys_major, SP, axis=1, tiled=True)
+    key_piece = jnp.concatenate(
+        lax.all_to_all(jnp.stack([keys_major] * lax.axis_size(SP)), SP, 0, 0), axis=1
+    )
     value_piece = lax.all_gather(values_major, SP, axis=1, tiled=True)
 
     def one_block(block_index, states):

time: 637 us -> 747 us (1.17)
  blocking collectives: 62.5 us -> 184 us
  waiting for transfers between devices: 34.9 us -> 0.04 us
  starting transfers between devices: 1.36 us -> 22.2 us
  local copies, waits for them, and re-layouts: 106 us -> 115 us
    unnamed x1, blocking collectives: 7.68 us -> 144 us
    all_gather x1 -> x0, waiting for transfers between devices: 34.8 us -> none  [per_device(): key_piece = lax.all_gather(keys_major, SP, axis=1, tiled=True)]
    all_to_all x0 -> x2, starting transfers between devices: none -> 20.9 us  [the longest x1 14.5 us: per_device(): lax.all_to_all(ssm_out, 'tp', split_axis=0, concat_axis=1, tiled=True)]
    all_to_all x1 -> x0, blocking collectives: 10.5 us -> none  [per_device(): lax.all_to_all(ssm_out, 'tp', split_axis=0, concat_axis=1, tiled=True)]
    all_to_all x0 -> x1, local copies, waits for them, and re-layouts: none -> 7.74 us  [per_device(): lax.all_to_all(jnp.stack([keys_major] * lax.axis_size(SP)), SP, 0, 0)]
  transfers between devices with their start and end apart: 4 -> 5, of which waited for: 1 -> 0; matrix products, arithmetic and copies ran while one was open for 12% -> 12% of each run, Pallas kernels for 0% -> 0%
where the time goes in v1:
time: 747 us; the launch traced here: 743 us
  matrix products  311 us (42%)
  blocking collectives  184 us (25%)
  local copies, waits for them, and re-layouts  115 us (15%)
  other arithmetic  50.6 us (7%)
  loops' own time  45 us (6%)
  starting transfers between devices  22.2 us (3%)
  between operations  14.6 us (2%)
    dot_general x64, matrix products, update(): jnp.einsum('hmqk,hke->hmqe', weights.astype(jnp.bfloat16), value_rows, pr...  195 us
    unnamed x1, blocking collectives  144 us
    dot_general x64, matrix products, update(): jnp.einsum('mqd,mkd->mqk', group_query, key_rows, preferred_element_type=...  80.2 us
    another operation x1, loops' own time, per_device(): lax.fori_loop(0, key_piece.shape[1] // KEY_BLOCK, one_block, start_states)  40.1 us
    slice x64, local copies, waits for them, and re-layouts, one_block(): group_pos[-1]  37.7 us
    all_gather x3, blocking collectives, prefix_by_axis(): lax.all_gather(part.astype(kind), axis)  28.3 us
    mul x64, local copies, waits for them, and re-layouts, update(): jnp.einsum('mqd,mkd->mqk', group_query, key_rows, preferred_element_type=...  20.7 us
    dot_general x8, matrix products, per_device(): jnp.dot(whole, weight, preferred_element_type=jnp.float32)  19.2 us
  transfers between devices with their start and end apart: 5, of which 0 were waited for; matrix products, arithmetic and copies ran while one was open for 12% of the time, Pallas kernels for 0%

profile of v1, /device:TPU:127, one launch (start us, length us, event | category | flops | bytes accessed | tf_op | source)
XLA Modules:
  0.0 742.9 jit_solution(6961739316583778211)
XLA Ops:
  18.0 5.5 all_to_all.48
  31.5 5.3 stack.2
  36.8 6.5 all-to-all-start.1
  54.3 144.3 %all-reduce.1 = bf16[32]{0:T(256)(128)(2,1)S(1)} all-reduce(bf16[32]{0:T(256)(128)(2,1)S(1)} %dynamic-update-slice), channel_id=3, replica_groups=mesh['sp_0'=4,'sp_1'=4,'fs'=4,'tp'=2] {'sp_1'}, use_global_device_ids=true, to_apply=%add.1 | all-reduce | flops 32 | bytes 128
  198.7 8.1 %all-gather.4 = bf16[4,1,8]{2,1,0:T(2,128)(2,1)S(1)} all-gather(bf16[1,1,8]{2,1,0:T(2,128)(2,1)S(1)} %get-tuple-element.351), channel_id=1, replica_groups=mesh['sp_0'=4,'sp_1'=4,'fs'=4,'tp'=2] {'sp_0'}, dimensions={0}, use_global_device_ids=true | all-gather | bytes 80 | tf_op jit(solution)/shard_map/all_gather | solution.py:57
  227.1 7.2 while.31
  235.5 10.1 %all-gather.2 = bf16[32,64,128]{2,1,0:T(8,128)(2,1)S(1)} all-gather(bf16[8,64,128]{2,1,0:T(8,128)(2,1)S(1)} %convert_element_type.242), channel_id=4, replica_groups=mesh['sp_0'=4,'sp_1'=4,'fs'=4,'tp'=2] {'sp_1'}, dimensions={0}, use_global_device_ids=true | all-gather | bytes 655360 | tf_op jit(solution)/shard_map/all_gather | solution.py:57
  246.5 10.2 %all_gather.38 = bf16[4,8,64,128]{3,2,1,0:T(8,128)(2,1)S(1)} all-gather(bf16[1,8,64,128]{3,2,1,0:T(8,128)(2,1)S(1)} %fusion.62), channel_id=1, replica_groups=mesh['sp_0'=4,'sp_1'=4,'fs'=4,'tp'=2] {'sp_0'}, dimensions={0}, use_global_device_ids=true | all-gather | bytes 655360 | tf_op jit(solution)/shard_map/all_gather | solution.py:57
  278.7 14.5 %all-to-all-start.3 = ((bf16[2,256,512]{1,2,0:T(8,128)(2,1)}), bf16[2,256,512]{1,2,0:T(8,128)(2,1)S(1)}, u32[]{:S(2)}, u32[]{:S(2)}) async-start(bf16[2,256,512]{1,2,0:T(8,128)(2,1)} %copy.128), calls=%async_computation.3 | async-start | bytes 1048576 | tf_op jit(solution)/shard_map/all_to_all | solution.py:270
  293.2 7.7 %copy.112 = bf16[16,4,512,128]{3,2,0,1:T(8,128)(2,1)} copy(bf16[16,4,512,128]{3,2,1,0:T(8,128)(2,1)} %all-to-all-done.1) | data formatting | bytes 16777216 | tf_op jit(solution)/shard_map/all_to_all | solution.py:138
  307.3 416.1 %while.30 = (s32[]{:T(128)}, f32[2,2,512]{2,1,0:T(2,128)S(1)}, f32[2,2,512]{2,1,0:T(2,128)S(1)}, f32[2,2,512,256]{3,2,1,0:T(8,128)}, s32[512]{0:T(512)S(1)}, /*i...) while((s32[]{:T(128)}, f32[2,2,512]{2,1,0:T(2,128)S(1)}, ...), condition=%wide.region_7.8_spmd, body=%wide.region_2.7_spmd.sunk | while | flops 204804224 | bytes 10801461 | solution.py:177
  315.0 5.3 conditional.2
  328.0 5.3 conditional.2
  341.0 5.3 conditional.2
  354.0 5.3 conditional.2
  367.0 5.3 conditional.2
  380.0 5.3 conditional.2
  393.0 5.3 conditional.2
  406.0 5.3 conditional.2
  419.0 5.3 conditional.2
  458.0 5.3 conditional.2
  510.0 5.3 conditional.2
  562.0 5.3 conditional.2
  705.1 5.3 conditional.2
  (1178 shorter events, 740.6 us)
Async XLA Ops:
  6.5 262.6 %copy-start = (bf16[2048,512]{1,0:T(8,128)(2,1)S(1)}, bf16[2048,512]{1,0:T(8,128)(2,1)}, u32[]{:S(2)}) copy-start(bf16[2048,512]{1,0:T(8,128)(2,1)} %param.31) | copy-start | bytes 6291460
  6.5 294.4 %all-gather.10.cloned.1.call-start = ((), (), s32[]{:S(2)}) async-start(), calls=%async_computation.5 | async-start | bytes 12582912 | tf_op jit(solution)/shard_map/all_gather | solution.py:74
  11.4 294.3 %all-gather.8.cloned.1.call-start = ((), (), s32[]{:S(2)}) async-start(), calls=%async_computation.4 | async-start | bytes 8912896 | tf_op jit(solution)/shard_map/all_gather | solution.py:140
  18.0 6.8 copy-start.25
  36.8 6.5 copy-start.27
  36.8 242.0 %all-to-all-start.1 = ((bf16[16,4,512,128]{3,2,1,0:T(8,128)(2,1)}), bf16[16,4,512,128]{3,2,1,0:T(8,128)(2,1)}, u32[]{:S(2)}, u32[]{:S(2)}) async-start(bf16[16,4,512,128]{3,2,1,0:T(8,128)(2,1)} %stack.2), calls=%async_computation.1 | async-start | bytes 16777216 | tf_op jit(solution)/shard_map/all_to_all | solution.py:138
  43.2 2.5 copy-start.3
  43.2 2.5 copy-start.28
  45.8 3.0 copy-start.8
  45.8 1.7 copy-start.26
  47.5 3.5 copy-start.29
  47.5 3.5 copy-start.14
  48.8 2.6 copy-start.15
  48.8 3.8 copy-start.30
  48.8 159.2 %copy-start.18 = (bf16[4,512]{1,0:T(4,128)(2,1)S(1)}, bf16[4,512]{1,0:T(4,128)(2,1)}, u32[]{:S(2)}) copy-start(bf16[4,512]{1,0:T(4,128)(2,1)} %param.36) | copy-start | bytes 12292
  48.8 159.2 %copy-start.19 = (bf16[4,256]{1,0:T(4,128)(2,1)S(1)}, bf16[4,256]{1,0:T(4,128)(2,1)}, u32[]{:S(2)}) copy-start(bf16[4,256]{1,0:T(4,128)(2,1)} %param.38) | copy-start | bytes 6148
  48.8 159.2 %copy-start.20 = (bf16[4,256]{1,0:T(4,128)(2,1)S(1)}, bf16[4,256]{1,0:T(4,128)(2,1)}, u32[]{:S(2)}) copy-start(bf16[4,256]{1,0:T(4,128)(2,1)} %param.37) | copy-start | bytes 6148
  49.7 166.6 %collective-permute-start = (bf16[3,1024]{0,1:T(8,128)(2,1)}, bf16[3,1024]{0,1:T(8,128)(2,1)}, u32[]{:S(2)}, u32[]{:S(2)}) collective-permute-start(bf16[3,1024]{0,1:T(8,128)(2,1)} %pad_maximum_fusion.1), channel_id=1, source_target_pairs={{0,8},{8,16},{16,24},{24,32},{32,40},{40,48},{48,56},{56,64},{64,7... | collective-permute-start | bytes 18440 | tf_op jit(solution)/shard_map/ppermute | solution.py:42
  51.4 162.9 %copy-start.10 = (f32[512,8]{0,1:T(8,128)}, f32[512,8]{0,1:T(8,128)S(1)}, u32[]{:S(2)}) copy-start(f32[512,8]{0,1:T(8,128)S(1)} %compare_select_fusion) | copy-start | bytes 49156
  278.7 22.2 %all-to-all-start.3 = ((bf16[2,256,512]{1,2,0:T(8,128)(2,1)}), bf16[2,256,512]{1,2,0:T(8,128)(2,1)S(1)}, u32[]{:S(2)}, u32[]{:S(2)}) async-start(bf16[2,256,512]{1,2,0:T(8,128)(2,1)} %copy.128), calls=%async_computation.3 | async-start | bytes 1048576 | tf_op jit(solution)/shard_map/all_to_all | solution.py:270
  305.7 1.5 copy-start.12
  307.3 416.1 %copy-start.24 = (f32[2]{0:T(128)S(1)}, f32[2]{0:T(128)}, u32[]{:S(2)}) copy-start(f32[2]{0:T(128)} %param.41) | copy-start | bytes 28
  723.4 2.1 copy-start.23
  730.8 5.3 copy-start.1
  (12 other events, 13.8 us)
Sparse Core Ops, SparseCore 0:
  11.5 24.0 all-gather.9
  37.7 175.0 all-gather.7
